TPU v7x, 32 devices: a whole 2x2x4 slice. The times are simulated.
32 devices in a mesh: sp: 8 (over z, y), tp: 4 (over x, core).
Axes of the slice: x: 2, y: 2, z: 4, core: 2. Of those that a mesh axis runs over, the one named last changes fastest.
Arguments:
- query_rows: bfloat16 [4096, 1024], P('sp', 'tp'), may hold values from -6 to 6
- key_rows: bfloat16 [4096, 512], P('sp', 'tp'), may hold values from -6 to 6
- value_rows: bfloat16 [4096, 512], P('sp', 'tp'), may hold values from -12 to 12
- query_gain: float32 [128], replicated, may hold values from 0.2 to 6.5
- key_gain: float32 [128], replicated, may hold values from 0.2 to 6.5
- residual: bfloat16 [4096, 2048], P(('sp', 'tp')), may hold values from -6 to 6
- out_weight: bfloat16 [1024, 2048], P('tp'), may hold values from -3 to 3
- mix_gain: float32 [2048], replicated, may hold values from 0.1 to 1.9
- gate_weight: bfloat16 [2048, 5632], P('sp', 'tp'), may hold values from -0.125 to 0.125
- up_weight: bfloat16 [2048, 5632], P('sp', 'tp'), may hold values from -0.125 to 0.125
- down_weight: bfloat16 [5632, 2048], P('tp', 'sp'), may hold values from -0.15625 to 0.15625
Outputs:
- layer_out: bfloat16 [4096, 2048], P(('sp', 'tp'))
All inputs are finite; a program needn't handle non-finite values.
Results may differ from a plain program's by a relative error of at most 0.015.
The roundings to bfloat16 on the way count: a program that leaves them out, or rounds other values in their place, can miss the bound.
Values may be sent and summed in bfloat16 or wider, within the bound.
A program may use at most 128 MiB of HBM per device.

v0:
```python
import jax
import jax.numpy as jnp
from jax import lax
from jax.sharding import PartitionSpec as P

GRID = 64
norm_eps = 1e-06
theta_base = 10000.0


def spin(halfway, angles):
    cosine = jnp.cos(angles)[:, None, :]
    sine_val = jnp.sin(angles)[:, None, :]
    quarter = halfway.shape[-1] // 2
    leading = halfway[..., :quarter]
    trailing = halfway[..., quarter:]
    return [leading * cosine - trailing * sine_val, trailing * cosine + leading * sine_val]


def rotate_grid(vectors, positions):
    head_dim = vectors.shape[-1]
    quarter = head_dim // 4
    frequency = jnp.power(
        theta_base, -2.0 * jnp.arange(quarter, dtype=jnp.float32) / (head_dim // 2)
    )
    row_angle = (positions // GRID).astype(jnp.float32)[:, None] * frequency
    col_angle = (positions % GRID).astype(jnp.float32)[:, None] * frequency
    lower_half = vectors[..., : 2 * quarter]
    upper_half = vectors[..., 2 * quarter :]
    return jnp.concatenate(spin(lower_half, row_angle) + spin(upper_half, col_angle), axis=-1)


def prepare_heads(raw_heads, head_gain, positions):
    floated = raw_heads.astype(jnp.float32)
    scaled = floated * lax.rsqrt(jnp.mean(floated * floated, axis=-1, keepdims=True) + norm_eps)
    return rotate_grid(scaled * head_gain, positions).astype(jnp.bfloat16)


def row_norm(row_data, row_gain):
    floated = row_data.astype(jnp.float32)
    scaled = floated * lax.rsqrt(jnp.mean(floated * floated, axis=-1, keepdims=True) + norm_eps)
    return (scaled * row_gain).astype(jnp.bfloat16)


def on_device(
    query_rows,
    key_rows,
    value_rows,
    query_gain,
    key_gain,
    residual,
    out_weight,
    mix_gain,
    gate_weight,
    up_weight,
    down_weight,
):
    tok_rows = query_rows.shape[0]
    head_dim = query_gain.shape[0]
    local_kv = key_rows.shape[1] // head_dim
    local_q = query_rows.shape[1] // head_dim
    group_size = local_q // local_kv
    positions = lax.axis_index("sp") * tok_rows + jnp.arange(tok_rows, dtype=jnp.int32)
    gate_whole, up_whole, down_whole = (
        lax.all_gather(gate_weight, "sp", axis=0, tiled=True),
        lax.all_gather(up_weight, "sp", axis=0, tiled=True),
        lax.all_gather(down_weight, "sp", axis=1, tiled=True),
    )
    q_heads = prepare_heads(query_rows.reshape(tok_rows, local_q, head_dim), query_gain, positions)
    q_stack = (
        q_heads.reshape(tok_rows, local_kv, group_size, head_dim)
        .transpose(1, 2, 0, 3)
        .reshape(local_kv, group_size * tok_rows, head_dim)
    )
    k_heads = prepare_heads(
        key_rows.reshape(tok_rows, local_kv, head_dim), key_gain, positions
    ).reshape(tok_rows, local_kv * head_dim)
    score_scale = head_dim ** (-0.5)
    start_state = (
        jnp.full((local_kv, group_size * tok_rows), -jnp.inf, jnp.float32),
        jnp.zeros((local_kv, group_size * tok_rows), jnp.float32),
        jnp.zeros((local_kv, group_size * tok_rows, head_dim), jnp.float32),
    )
    key_piece = lax.all_gather(k_heads, "sp", axis=0, tiled=True)
    value_piece = lax.all_gather(value_rows, "sp", axis=0, tiled=True)
    count_rows = key_piece.shape[0]
    key_blocks = key_piece.reshape(count_rows // tok_rows, tok_rows, local_kv, head_dim).transpose(
        0, 2, 1, 3
    )
    value_blocks = value_piece.reshape(
        count_rows // tok_rows, tok_rows, local_kv, head_dim
    ).transpose(0, 2, 1, 3)

    def inner(state, blocks):
        key_block, value_block = blocks
        running_max, running_sum, weighted = state
        scores = (
            jnp.einsum("kqd,ksd->kqs", q_stack, key_block, preferred_element_type=jnp.float32)
            * score_scale
        )
        new_max = jnp.maximum(running_max, jnp.max(scores, axis=-1))
        weights = jnp.exp(scores - new_max[..., None])
        factor = jnp.exp(running_max - new_max)
        running_sum = running_sum * factor + jnp.sum(weights, axis=-1)
        weighted = weighted * factor[..., None] + jnp.einsum(
            "kqs,ksd->kqd",
            weights.astype(jnp.bfloat16),
            value_block,
            preferred_element_type=jnp.float32,
        )
        return ((new_max, running_sum, weighted), None)

    result, unused = lax.scan(inner, start_state, (key_blocks, value_blocks))
    final_max, final_sum, weighted = result
    attended = (weighted / final_sum[..., None]).reshape(local_kv, group_size, tok_rows, head_dim)
    attended = (
        attended.transpose(2, 0, 1, 3).reshape(tok_rows, local_q * head_dim).astype(jnp.bfloat16)
    )
    attn_sum = lax.psum_scatter(
        jnp.dot(attended, out_weight, preferred_element_type=jnp.float32).astype(jnp.bfloat16),
        "tp",
        scatter_dimension=0,
        tiled=True,
    ).astype(jnp.float32)
    own_rows = (residual.astype(jnp.float32) + attn_sum).astype(jnp.bfloat16)
    normed_all = lax.all_gather(row_norm(own_rows, mix_gain), "tp", axis=0, tiled=True)
    gate_act = jnp.dot(normed_all, gate_whole, preferred_element_type=jnp.float32)
    up_act = jnp.dot(normed_all, up_whole, preferred_element_type=jnp.float32)
    hidden = (jax.nn.silu(gate_act) * up_act).astype(jnp.bfloat16)
    unit_sum = lax.psum_scatter(
        jnp.dot(hidden, down_whole, preferred_element_type=jnp.float32).astype(jnp.bfloat16),
        "tp",
        scatter_dimension=0,
        tiled=True,
    ).astype(jnp.float32)
    return (own_rows.astype(jnp.float32) + 0.5 * unit_sum).astype(jnp.bfloat16)


def solution(mesh):
    placed = (
        P("sp", "tp"),
        P("sp", "tp"),
        P("sp", "tp"),
        P(),
        P(),
        P(("sp", "tp"), None),
        P("tp", None),
        P(),
        P("sp", "tp"),
        P("sp", "tp"),
        P("tp", "sp"),
    )
    return jax.shard_map(
        on_device, mesh=mesh, in_specs=placed, out_specs=P(("sp", "tp"), None), check_vma=False
    )
```

profile of v0, /device:TPU:0, one launch (start us, length us, event | category | flops | bytes accessed | tf_op | source)
XLA Modules:
  0.0 523.7 jit_solution(12080952115448605212)
XLA Ops:
  12.5 1.9 multiply_cosine_fusion.1
  15.1 1.8 fusion.26
  16.9 1.6 maximum_bitcast_fusion
  18.5 33.5 %all-gather.7.cloned.1.call-done = bf16[4096,128]{0,1:T(8,128)(2,1)} async-done(((bf16[512,128]{0,1:T(8,128)(2,1)}), bf16[4096,128]{0,1:T(8,128)(2,1)}) %all-gather.7.cloned.1.call-update) | async-done | bytes 1048592 | tf_op jit(solution)/shard_map/all_gather | solution.py:84
  52.0 2.3 copy.24
  54.3 39.2 %all-gather.9.cloned.1.call-done = bf16[4096,128]{1,0:T(8,128)(2,1)} async-done(((bf16[512,128]{1,0:T(8,128)(2,1)}), bf16[4096,128]{1,0:T(8,128)(2,1)}) %all-gather.9.cloned.1.call-update) | async-done | bytes 1048592 | tf_op jit(solution)/shard_map/all_gather | solution.py:85
  93.5 37.9 %while.15 = (s32[]{:T(128)}, f32[1,1024]{1,0:T(1,128)S(1)}, f32[1,1024]{1,0:T(1,128)S(1)}, f32[1,1024,128]{2,1,0:T(8,128)}, bf16[8,1,512,128]{3,2,1,0:T(8,128)(2...) while((s32[]{:T(128)}, f32[1,1024]{1,0:T(1,128)S(1)}, ...), condition=%wide.region_5.6_spmd.clone, body=%wide.region_2.5_spmd.clone.sunk | while | flops 273028096 | bytes 12125345 | solution.py:113
  105.3 1.5 fusion.75
  110.1 1.5 fusion.75
  114.8 1.5 fusion.75
  119.5 1.5 fusion.75
  124.3 1.5 fusion.75
  129.0 1.5 fusion.75
  132.8 2.1 convolution_convert_fusion
  134.9 30.0 %reduce-scatter.3.cloned.1.call-done = bf16[128,2048]{1,0:T(8,128)(2,1)} async-done(((bf16[512,2048]{1,0:T(8,128)(2,1)}), bf16[128,2048]{1,0:T(8,128)(2,1)}) %reduce-scatter.3.cloned.1.call-update) | async-done | bytes 524304 | tf_op jit(solution)/shard_map/reduce_scatter | solution.py:119
  166.2 2.0 fusion.21
  170.4 20.6 %all-gather.11.cloned.1.call-done = bf16[512,2048]{1,0:T(8,128)(2,1)} async-done(((bf16[128,2048]{1,0:T(8,128)(2,1)}), bf16[512,2048]{1,0:T(8,128)(2,1)}) %all-gather.11.cloned.1.call-update) | async-done | bytes 2097168 | tf_op jit(solution)/shard_map/all_gather | solution.py:126
  191.0 94.4 %all-gather.13.cloned.1.call-done = bf16[2048,1408]{1,0:T(8,128)(2,1)} async-done(((bf16[256,1408]{1,0:T(8,128)(2,1)}), bf16[2048,1408]{1,0:T(8,128)(2,1)}) %all-gather.13.cloned.1.call-update) | async-done | bytes 5767184 | tf_op jit(solution)/shard_map/all_gather | solution.py:65
  285.4 8.2 %fusion.56 = f32[512,1408]{1,0:T(8,128)} fusion(bf16[512,2048]{1,0:T(8,128)(2,1)} %all-gather.11.cloned.1.call-done, bf16[2048,1408]{1,0:T(8,128)(2,1)} %all-gather.13.cloned.1.call-done), kind=kOutput, calls=%fused_computation.99 | convolution fusion | flops 2952790016 | bytes 10747904 | tf_op jit(solution)/shard_map/dot_general | solution.py:127
  293.6 84.3 %all-gather.15.cloned.1.call-done = bf16[2048,1408]{1,0:T(8,128)(2,1)} async-done(((bf16[256,1408]{1,0:T(8,128)(2,1)}), bf16[2048,1408]{1,0:T(8,128)(2,1)}) %all-gather.15.cloned.1.call-update) | async-done | bytes 5767184 | tf_op jit(solution)/shard_map/all_gather | solution.py:66
  377.9 93.4 %all-gather.17.cloned.1.call-done = bf16[1408,2048]{1,0:T(8,128)(2,1)} async-done(((bf16[1408,256]{1,0:T(8,128)(2,1)}), bf16[1408,2048]{1,0:T(8,128)(2,1)}) %all-gather.17.cloned.1.call-update) | async-done | bytes 5767184 | tf_op jit(solution)/shard_map/all_gather | solution.py:67
  471.3 14.0 %convolution_convert_fusion.1 = bf16[512,2048]{1,0:T(8,128)(2,1)} fusion(bf16[1408,2048]{1,0:T(8,128)(2,1)} %all-gather.17.cloned.1.call-done, bf16[512,2048]{1,0:T(8,128)(2,1)} %all-gather.11.cloned.1.call-done, bf16[2048,1408]{1,0:T(8,128)(2,1)} %all-gather.15.cloned.1.call-done, f32[512,1408]{1,0:T(8,128)} %fusion.56), kind=kOutput, calls=%fused_computation.27 | convolution fusion | flops 5910953984 | bytes 18612224 | tf_op jit(solution)/shard_map/dot_general | solution.py:131
  485.3 29.5 %reduce-scatter.5.cloned.1.call-done = bf16[128,2048]{1,0:T(8,128)(2,1)} async-done(((bf16[512,2048]{1,0:T(8,128)(2,1)}), bf16[128,2048]{1,0:T(8,128)(2,1)}) %reduce-scatter.5.cloned.1.call-update) | async-done | bytes 524304 | tf_op jit(solution)/shard_map/reduce_scatter | solution.py:130
  514.8 2.1 fusion.22
  (120 shorter events, 39.8 us)
Async XLA Ops:
  6.5 126.2 %copy-start = (bf16[256,2048]{1,0:T(8,128)(2,1)S(1)}, bf16[256,2048]{1,0:T(8,128)(2,1)}, u32[]{:S(2)}) copy-start(bf16[256,2048]{1,0:T(8,128)(2,1)} %param.19) | copy-start | bytes 3145732
  6.5 45.5 %all-gather.7.cloned.1.call-start = ((), (), s32[]{:S(2)}) async-start(), calls=%async_computation.2 | async-start | bytes 1179648 | tf_op jit(solution)/shard_map/all_gather | solution.py:84
  8.5 5.9 %copy-start.6 = (f32[128]{0:T(128)S(1)}, f32[128]{0:T(128)}, u32[]{:S(2)}) copy-start(f32[128]{0:T(128)} %param.16) | copy-start | bytes 1540
  9.7 83.7 %all-gather.9.cloned.1.call-start = ((), (), s32[]{:S(2)}) async-start(), calls=%async_computation.3 | async-start | bytes 1179648 | tf_op jit(solution)/shard_map/all_gather | solution.py:85
  10.5 154.4 %reduce-scatter.3.cloned.1.call-start = ((), (), s32[]{:S(2)}) async-start(), calls=%async_computation.4 | async-start | bytes 2621440 | tf_op jit(solution)/shard_map/reduce_scatter | solution.py:119
  94.8 1.0 copy-start.1
  97.4 0.8 copy-start.2
  99.6 1.0 copy-start.1
  102.2 0.8 copy-start.2
  104.3 1.0 copy-start.1
  109.0 1.0 copy-start.1
  113.8 1.0 copy-start.1
  116.3 0.8 copy-start.2
  118.5 1.0 copy-start.1
  123.2 1.0 copy-start.1
  128.0 1.0 copy-start.1
  134.8 30.0 %copy-start.3 = (bf16[128,2048]{1,0:T(8,128)(2,1)S(1)}, bf16[128,2048]{1,0:T(8,128)(2,1)}, u32[]{:S(2)}) copy-start(bf16[128,2048]{1,0:T(8,128)(2,1)} %param.18) | copy-start | bytes 1572868
  134.8 31.4 %copy-start.5 = (f32[2048]{0:T(1024)S(1)}, f32[2048]{0:T(1024)}, u32[]{:S(2)}) copy-start(f32[2048]{0:T(1024)} %param.20) | copy-start | bytes 24580
  134.9 56.1 %all-gather.11.cloned.1.call-start = ((), (), s32[]{:S(2)}) async-start(), calls=%async_computation.5 | async-start | bytes 2621440 | tf_op jit(solution)/shard_map/all_gather | solution.py:126
  168.3 117.1 %all-gather.13.cloned.1.call-start = ((), (), s32[]{:S(2)}) async-start(), calls=%async_computation.6 | async-start | bytes 6488064 | tf_op jit(solution)/shard_map/all_gather | solution.py:65
  168.9 209.1 %all-gather.15.cloned.1.call-start = ((), (), s32[]{:S(2)}) async-start(), calls=%async_computation.7 | async-start | bytes 6488064 | tf_op jit(solution)/shard_map/all_gather | solution.py:66
  169.4 301.9 %all-gather.17.cloned.1.call-start = ((), (), s32[]{:S(2)}) async-start(), calls=%async_computation.8 | async-start | bytes 6488064 | tf_op jit(solution)/shard_map/all_gather | solution.py:67
  170.2 344.6 %reduce-scatter.5.cloned.1.call-start = ((), (), s32[]{:S(2)}) async-start(), calls=%async_computation.9 | async-start | bytes 2621440 | tf_op jit(solution)/shard_map/reduce_scatter | solution.py:130
  485.3 29.5 %copy-start.4 = (bf16[128,2048]{1,0:T(8,128)(2,1)S(1)}, bf16[128,2048]{1,0:T(8,128)(2,1)}, u32[]{:S(2)}) copy-start(bf16[128,2048]{1,0:T(8,128)(2,1)} %reduce-scatter.3.cloned.1.call-done) | copy-start | bytes 1572868
  (5 other events, 4.0 us)
Sparse Core Ops, SparseCore 0:
  9.9 42.1 all-gather.6
  54.2 39.2 all-gather.8
  135.0 29.8 reduce-scatter.2
  168.4 22.5 all-gather.10
  193.0 92.3 all-gather.12
  287.4 90.4 all-gather.14
  380.0 91.2 all-gather.16
  485.4 29.3 reduce-scatter.4
where the time goes:
time: 525 us; the launch traced here: 524 us
  waiting for transfers between devices  427 us (81%)
  matrix products  47.2 us (9%)
  other arithmetic  18.6 us (4%)
  local copies, waits for them, and re-layouts  16.1 us (3%)
  between operations  13.6 us (3%)
    all_gather x1, waiting for transfers between devices, on_device(): lax.all_gather(gate_weight, 'sp', axis=0, tiled=True)  94.4 us
    all_gather x1, waiting for transfers between devices, on_device(): lax.all_gather(down_weight, 'sp', axis=1, tiled=True)  93.4 us
    all_gather x1, waiting for transfers between devices, on_device(): lax.all_gather(up_weight, 'sp', axis=0, tiled=True)  84.3 us
    all_gather x1, waiting for transfers between devices, on_device(): value_piece = lax.all_gather(value_rows, 'sp', axis=0, tiled=True)  39.2 us
    all_gather x1, waiting for transfers between devices, on_device(): key_piece = lax.all_gather(k_heads, 'sp', axis=0, tiled=True)  33.5 us
    reduce_scatter x1, waiting for transfers between devices, on_device(): lax.psum_scatter(jnp.dot(attended, out_weight, preferred_element_type=jnp...  30 us
    reduce_scatter x1, waiting for transfers between devices, on_device(): lax.psum_scatter(jnp.dot(hidden, down_whole, preferred_element_type=jnp.f...  29.5 us
    all_gather x1, waiting for transfers between devices, on_device(): lax.all_gather(row_norm(own_rows, mix_gain), 'tp', axis=0, tiled=True)  20.6 us
  transfers between devices with their start and end apart: 8, of which 8 were waited for; matrix products, arithmetic and copies ran while one was open for 4% of the time, Pallas kernels for 0%

commit v1 on v0

--- a/solution.py
+++ b/solution.py
@@ -82,7 +82,12 @@
         jnp.zeros((local_kv, group_size * tok_rows, head_dim), jnp.float32),
     )
     key_piece = lax.all_gather(k_heads, "sp", axis=0, tiled=True)
-    value_piece = lax.all_gather(value_rows, "sp", axis=0, tiled=True)
+    ring = [value_rows]
+    for hop in range(7):
+        ring.append(lax.ppermute(ring[-1], "sp", [(dev, (dev + 1) % 8) for dev in range(8)]))
+    value_piece = jnp.roll(
+        jnp.concatenate(ring[::-1], axis=0), (lax.axis_index("sp") + 1) * ring[0].shape[0], axis=0
+    )
     count_rows = key_piece.shape[0]
     key_blocks = key_piece.reshape(count_rows // tok_rows, tok_rows, local_kv, head_dim).transpose(
         0, 2, 1, 3

time: 525 us -> 498 us (0.949)
  waiting for transfers between devices: 427 us -> 396 us
    ppermute x0 -> x7, waiting for transfers between devices: none -> 43.9 us  [on_device(): lax.ppermute(ring[-1], 'sp', [(dev, (dev + 1) % 8) for dev in range(8)])]
    all_gather x1 -> x0, waiting for transfers between devices: 39.2 us -> none  [on_device(): value_piece = lax.all_gather(value_rows, 'sp', axis=0, tiled=True)]
    all_gather x1, waiting for transfers between devices: 33.5 us -> 0.01 us  [on_device(): key_piece = lax.all_gather(k_heads, 'sp', axis=0, tiled=True)]
  transfers between devices with their start and end apart: 8 -> 14, of which waited for: 8 -> 13; matrix products, arithmetic and copies ran while one was open for 4% -> 4% of each run, Pallas kernels for 0% -> 0%
where the time goes in v1:
time: 498 us; the launch traced here: 497 us
  waiting for transfers between devices  396 us (80%)
  matrix products  47.2 us (9%)
  other arithmetic  18.6 us (4%)
  local copies, waits for them, and re-layouts  17.4 us (3%)
  between operations  13.8 us (3%)
    all_gather x1, waiting for transfers between devices, on_device(): lax.all_gather(gate_weight, 'sp', axis=0, tiled=True)  94.4 us
    all_gather x1, waiting for transfers between devices, on_device(): lax.all_gather(down_weight, 'sp', axis=1, tiled=True)  93.2 us
    all_gather x1, waiting for transfers between devices, on_device(): lax.all_gather(up_weight, 'sp', axis=0, tiled=True)  84.3 us
    ppermute x7, waiting for transfers between devices, on_device(): lax.ppermute(ring[-1], 'sp', [(dev, (dev + 1) % 8) for dev in range(8)])  43.9 us
    reduce_scatter x1, waiting for transfers between devices, on_device(): lax.psum_scatter(jnp.dot(hidden, down_whole, preferred_element_type=jnp.f...  29.5 us
    reduce_scatter x1, waiting for transfers between devices, on_device(): lax.psum_scatter(jnp.dot(attended, out_weight, preferred_element_type=jnp...  28.6 us
    all_gather x1, waiting for transfers between devices, on_device(): lax.all_gather(row_norm(own_rows, mix_gain), 'tp', axis=0, tiled=True)  20.7 us
    dot_general x1, matrix products, on_device(): jnp.dot(hidden, down_whole, preferred_element_type=jnp.float32)  13.9 us
  transfers between devices with their start and end apart: 14, of which 13 were waited for; matrix products, arithmetic and copies ran while one was open for 4% of the time, Pallas kernels for 0%

profile of v1, /device:TPU:0, one launch (start us, length us, event | category | flops | bytes accessed | tf_op | source)
XLA Modules:
  0.0 497.1 jit_solution(14962767185020572494)
XLA Ops:
  6.5 3.0 collective-permute-start
  11.4 4.9 collective-permute-done
  18.8 5.1 %collective-permute-done.1 = bf16[512,128]{1,0:T(8,128)(2,1)S(1)} collective-permute-done((bf16[512,128]{1,0:T(8,128)(2,1)S(1)}, bf16[512,128]{1,0:T(8,128)(2,1)S(1)}, u32[]{:S(2)}, u32[]{:S(2)}) %collective-permute-start.1) | collective-permute-done | bytes 131104 | tf_op jit(solution)/shard_map/ppermute | solution.py:87
  24.6 7.1 %collective-permute-done.2 = bf16[512,128]{1,0:T(8,128)(2,1)S(1)} collective-permute-done((bf16[512,128]{1,0:T(8,128)(2,1)S(1)}, bf16[512,128]{1,0:T(8,128)(2,1)S(1)}, u32[]{:S(2)}, u32[]{:S(2)}) %collective-permute-start.2) | collective-permute-done | bytes 131104 | tf_op jit(solution)/shard_map/ppermute | solution.py:87
  31.8 8.0 %collective-permute-done.3 = bf16[512,128]{1,0:T(8,128)(2,1)S(1)} collective-permute-done((bf16[512,128]{1,0:T(8,128)(2,1)S(1)}, bf16[512,128]{1,0:T(8,128)(2,1)S(1)}, u32[]{:S(2)}, u32[]{:S(2)}) %collective-permute-start.3) | collective-permute-done | bytes 131104 | tf_op jit(solution)/shard_map/ppermute | solution.py:87
  40.5 7.0 %collective-permute-done.4 = bf16[512,128]{1,0:T(8,128)(2,1)S(1)} collective-permute-done((bf16[512,128]{1,0:T(8,128)(2,1)S(1)}, bf16[512,128]{1,0:T(8,128)(2,1)S(1)}, u32[]{:S(2)}, u32[]{:S(2)}) %collective-permute-start.4) | collective-permute-done | bytes 131104 | tf_op jit(solution)/shard_map/ppermute | solution.py:87
  47.5 1.9 multiply_cosine_fusion.1
  49.4 7.6 %collective-permute-done.5 = bf16[512,128]{1,0:T(8,128)(2,1)S(1)} collective-permute-done((bf16[512,128]{1,0:T(8,128)(2,1)S(1)}, bf16[512,128]{1,0:T(8,128)(2,1)S(1)}, u32[]{:S(2)}, u32[]{:S(2)}) %collective-permute-start.5) | collective-permute-done | bytes 131104 | tf_op jit(solution)/shard_map/ppermute | solution.py:87
  57.0 1.8 fusion.26
  58.8 1.6 maximum_bitcast_fusion
  60.5 4.1 collective-permute-done.6
  66.1 2.3 copy.24
  68.4 37.9 %while.15 = (s32[]{:T(128)}, f32[1,1024]{1,0:T(1,128)S(1)}, f32[1,1024]{1,0:T(1,128)S(1)}, f32[1,1024,128]{2,1,0:T(8,128)}, bf16[8,1,512,128]{3,2,1,0:T(8,128)(2...) while((s32[]{:T(128)}, f32[1,1024]{1,0:T(1,128)S(1)}, ...), condition=%wide.region_5.6_spmd.clone, body=%wide.region_2.5_spmd.clone.sunk | while | flops 273028096 | bytes 12125345 | solution.py:118
  107.7 2.1 convolution_convert_fusion
  109.8 28.6 %reduce-scatter.3.cloned.1.call-done = bf16[128,2048]{1,0:T(8,128)(2,1)} async-done(((bf16[512,2048]{1,0:T(8,128)(2,1)}), bf16[128,2048]{1,0:T(8,128)(2,1)}) %reduce-scatter.3.cloned.1.call-update) | async-done | bytes 524304 | tf_op jit(solution)/shard_map/reduce_scatter | solution.py:124
  139.8 2.0 fusion.21
  143.8 20.7 %all-gather.8.cloned.1.call-done = bf16[512,2048]{1,0:T(8,128)(2,1)} async-done(((bf16[128,2048]{1,0:T(8,128)(2,1)}), bf16[512,2048]{1,0:T(8,128)(2,1)}) %all-gather.8.cloned.1.call-update) | async-done | bytes 2097168 | tf_op jit(solution)/shard_map/all_gather | solution.py:131
  164.5 94.4 %all-gather.10.cloned.1.call-done = bf16[2048,1408]{1,0:T(8,128)(2,1)} async-done(((bf16[256,1408]{1,0:T(8,128)(2,1)}), bf16[2048,1408]{1,0:T(8,128)(2,1)}) %all-gather.10.cloned.1.call-update) | async-done | bytes 5767184 | tf_op jit(solution)/shard_map/all_gather | solution.py:65
  258.9 8.2 %fusion.56 = f32[512,1408]{1,0:T(8,128)} fusion(bf16[512,2048]{1,0:T(8,128)(2,1)} %all-gather.8.cloned.1.call-done, bf16[2048,1408]{1,0:T(8,128)(2,1)} %all-gather.10.cloned.1.call-done), kind=kOutput, calls=%fused_computation.116 | convolution fusion | flops 2952790016 | bytes 10747904 | tf_op jit(solution)/shard_map/dot_general | solution.py:132
  267.2 84.3 %all-gather.12.cloned.1.call-done = bf16[2048,1408]{1,0:T(8,128)(2,1)} async-done(((bf16[256,1408]{1,0:T(8,128)(2,1)}), bf16[2048,1408]{1,0:T(8,128)(2,1)}) %all-gather.12.cloned.1.call-update) | async-done | bytes 5767184 | tf_op jit(solution)/shard_map/all_gather | solution.py:66
  351.5 93.2 %all-gather.14.cloned.1.call-done = bf16[1408,2048]{1,0:T(8,128)(2,1)} async-done(((bf16[1408,256]{1,0:T(8,128)(2,1)}), bf16[1408,2048]{1,0:T(8,128)(2,1)}) %all-gather.14.cloned.1.call-update) | async-done | bytes 5767184 | tf_op jit(solution)/shard_map/all_gather | solution.py:67
  444.7 13.9 %convolution_convert_fusion.1 = bf16[512,2048]{1,0:T(8,128)(2,1)} fusion(bf16[1408,2048]{1,0:T(8,128)(2,1)} %all-gather.14.cloned.1.call-done, bf16[512,2048]{1,0:T(8,128)(2,1)} %all-gather.8.cloned.1.call-done, bf16[2048,1408]{1,0:T(8,128)(2,1)} %all-gather.12.cloned.1.call-done, f32[512,1408]{1,0:T(8,128)} %fusion.56), kind=kOutput, calls=%fused_computation.27 | convolution fusion | flops 5910953984 | bytes 18612224 | tf_op jit(solution)/shard_map/dot_general | solution.py:136
  458.7 29.5 %reduce-scatter.5.cloned.1.call-done = bf16[128,2048]{1,0:T(8,128)(2,1)} async-done(((bf16[512,2048]{1,0:T(8,128)(2,1)}), bf16[128,2048]{1,0:T(8,128)(2,1)}) %reduce-scatter.5.cloned.1.call-update) | async-done | bytes 524304 | tf_op jit(solution)/shard_map/reduce_scatter | solution.py:135
  488.2 2.1 fusion.22
  (150 shorter events, 49.3 us)
Async XLA Ops:
  6.5 101.1 %copy-start = (bf16[256,2048]{1,0:T(8,128)(2,1)S(1)}, bf16[256,2048]{1,0:T(8,128)(2,1)}, u32[]{:S(2)}) copy-start(bf16[256,2048]{1,0:T(8,128)(2,1)} %param.19) | copy-start | bytes 3145732
  6.5 33.3 %copy-start.7 = (f32[128]{0:T(128)S(1)}, f32[128]{0:T(128)}, u32[]{:S(2)}) copy-start(f32[128]{0:T(128)} %param.16) | copy-start | bytes 1540
  6.5 59.6 %all-gather.6.cloned.1.call-start = ((), (), s32[]{:S(2)}) async-start(), calls=%async_computation.2 | async-start | bytes 1179648 | tf_op jit(solution)/shard_map/all_gather | solution.py:84
  6.5 9.7 %collective-permute-start = (bf16[512,128]{1,0:T(8,128)(2,1)}, bf16[512,128]{1,0:T(8,128)(2,1)S(1)}, u32[]{:S(2)}, u32[]{:S(2)}) collective-permute-start(bf16[512,128]{1,0:T(8,128)(2,1)} %param.15), channel_id=1, source_target_pairs={{0,4},{4,8},{8,12},{12,16},{16,20},{20,24},{24,28},{28,0},{1,5},{5... | collective-permute-start | bytes 393224 | tf_op jit(solution)/shard_map/ppermute | solution.py:87
  16.3 7.7 %collective-permute-start.1 = (bf16[512,128]{1,0:T(8,128)(2,1)S(1)}, bf16[512,128]{1,0:T(8,128)(2,1)S(1)}, u32[]{:S(2)}, u32[]{:S(2)}) collective-permute-start(bf16[512,128]{1,0:T(8,128)(2,1)S(1)} %collective-permute-done), channel_id=1, source_target_pairs={{0,4},{4,8},{8,12},{12,16},{16,20},{20,24},{24,28},{28,0},{1,5},{5... | collective-permute-start | bytes 393224 | tf_op jit(solution)/shard_map/ppermute | solution.py:87
  17.5 120.9 %reduce-scatter.3.cloned.1.call-start = ((), (), s32[]{:S(2)}) async-start(), calls=%async_computation.3 | async-start | bytes 2621440 | tf_op jit(solution)/shard_map/reduce_scatter | solution.py:124
  23.9 7.8 %collective-permute-start.2 = (bf16[512,128]{1,0:T(8,128)(2,1)S(1)}, bf16[512,128]{1,0:T(8,128)(2,1)S(1)}, u32[]{:S(2)}, u32[]{:S(2)}) collective-permute-start(bf16[512,128]{1,0:T(8,128)(2,1)S(1)} %collective-permute-done.1), channel_id=1, source_target_pairs={{0,4},{4,8},{8,12},{12,16},{16,20},{20,24},{24,28},{28,0},{1,5},{5... | collective-permute-start | bytes 393224 | tf_op jit(solution)/shard_map/ppermute | solution.py:87
  31.7 8.1 %collective-permute-start.3 = (bf16[512,128]{1,0:T(8,128)(2,1)S(1)}, bf16[512,128]{1,0:T(8,128)(2,1)S(1)}, u32[]{:S(2)}, u32[]{:S(2)}) collective-permute-start(bf16[512,128]{1,0:T(8,128)(2,1)S(1)} %collective-permute-done.2), channel_id=1, source_target_pairs={{0,4},{4,8},{8,12},{12,16},{16,20},{20,24},{24,28},{28,0},{1,5},{5... | collective-permute-start | bytes 393224 | tf_op jit(solution)/shard_map/ppermute | solution.py:87
  39.8 7.7 %collective-permute-start.4 = (bf16[512,128]{1,0:T(8,128)(2,1)S(1)}, bf16[512,128]{1,0:T(8,128)(2,1)S(1)}, u32[]{:S(2)}, u32[]{:S(2)}) collective-permute-start(bf16[512,128]{1,0:T(8,128)(2,1)S(1)} %collective-permute-done.3), channel_id=1, source_target_pairs={{0,4},{4,8},{8,12},{12,16},{16,20},{20,24},{24,28},{28,0},{1,5},{5... | collective-permute-start | bytes 393224 | tf_op jit(solution)/shard_map/ppermute | solution.py:87
  47.5 9.5 %collective-permute-start.5 = (bf16[512,128]{1,0:T(8,128)(2,1)S(1)}, bf16[512,128]{1,0:T(8,128)(2,1)S(1)}, u32[]{:S(2)}, u32[]{:S(2)}) collective-permute-start(bf16[512,128]{1,0:T(8,128)(2,1)S(1)} %collective-permute-done.4), channel_id=1, source_target_pairs={{0,4},{4,8},{8,12},{12,16},{16,20},{20,24},{24,28},{28,0},{1,5},{5... | collective-permute-start | bytes 393224 | tf_op jit(solution)/shard_map/ppermute | solution.py:87
  56.9 7.7 %collective-permute-start.6 = (bf16[512,128]{1,0:T(8,128)(2,1)S(1)}, bf16[512,128]{1,0:T(8,128)(2,1)S(1)}, u32[]{:S(2)}, u32[]{:S(2)}) collective-permute-start(bf16[512,128]{1,0:T(8,128)(2,1)S(1)} %collective-permute-done.5), channel_id=1, source_target_pairs={{0,4},{4,8},{8,12},{12,16},{16,20},{20,24},{24,28},{28,0},{1,5},{5... | collective-permute-start | bytes 393224 | tf_op jit(solution)/shard_map/ppermute | solution.py:87
  58.7 6.1 %copy-start.5 = (bf16[512,128]{1,0:T(8,128)(2,1)S(1)}, bf16[512,128]{1,0:T(8,128)(2,1)}, u32[]{:S(2)}) copy-start(bf16[512,128]{1,0:T(8,128)(2,1)} %param.15) | copy-start | bytes 393220
  79.2 1.0 copy-start.1
  84.0 1.0 copy-start.1
  88.7 1.0 copy-start.1
  93.4 1.0 copy-start.1
  109.7 28.7 %copy-start.3 = (bf16[128,2048]{1,0:T(8,128)(2,1)S(1)}, bf16[128,2048]{1,0:T(8,128)(2,1)}, u32[]{:S(2)}) copy-start(bf16[128,2048]{1,0:T(8,128)(2,1)} %param.18) | copy-start | bytes 1572868
  109.7 30.0 %copy-start.6 = (f32[2048]{0:T(1024)S(1)}, f32[2048]{0:T(1024)}, u32[]{:S(2)}) copy-start(f32[2048]{0:T(1024)} %param.20) | copy-start | bytes 24580
  109.8 54.8 %all-gather.8.cloned.1.call-start = ((), (), s32[]{:S(2)}) async-start(), calls=%async_computation.4 | async-start | bytes 2621440 | tf_op jit(solution)/shard_map/all_gather | solution.py:131
  141.8 117.1 %all-gather.10.cloned.1.call-start = ((), (), s32[]{:S(2)}) async-start(), calls=%async_computation.5 | async-start | bytes 6488064 | tf_op jit(solution)/shard_map/all_gather | solution.py:65
  142.4 209.1 %all-gather.12.cloned.1.call-start = ((), (), s32[]{:S(2)}) async-start(), calls=%async_computation.6 | async-start | bytes 6488064 | tf_op jit(solution)/shard_map/all_gather | solution.py:66
  143.0 301.7 %all-gather.14.cloned.1.call-start = ((), (), s32[]{:S(2)}) async-start(), calls=%async_computation.7 | async-start | bytes 6488064 | tf_op jit(solution)/shard_map/all_gather | solution.py:67
  143.6 344.6 %reduce-scatter.5.cloned.1.call-start = ((), (), s32[]{:S(2)}) async-start(), calls=%async_computation.8 | async-start | bytes 2621440 | tf_op jit(solution)/shard_map/reduce_scatter | solution.py:135
  458.7 29.5 %copy-start.4 = (bf16[128,2048]{1,0:T(8,128)(2,1)S(1)}, bf16[128,2048]{1,0:T(8,128)(2,1)}, u32[]{:S(2)}) copy-start(bf16[128,2048]{1,0:T(8,128)(2,1)} %reduce-scatter.3.cloned.1.call-done) | copy-start | bytes 1572868
  (12 other events, 10.5 us)
Sparse Core Ops, SparseCore 0:
  17.7 43.8 all-gather.5
  109.9 28.5 reduce-scatter.2
  141.9 22.5 all-gather.7
  166.6 92.3 all-gather.9
  261.0 90.4 all-gather.11
  353.4 91.2 all-gather.13
  458.8 29.3 reduce-scatter.4
